TPU v7x, 32 devices: a whole 2x2x4 slice. The times are simulated.
32 devices in a mesh: grp: 2 (over y), fs: 4 (over z), tp: 4 (over x, core).
Axes of the slice: x: 2, y: 2, z: 4, core: 2. Of those that a mesh axis runs over, the one named last changes fastest.
Arguments:
- tokens: bfloat16 [3072, 2048], P(('grp', 'fs'), 'tp'), parts along dimension 0, may hold values from -6 to 6
- norm_gain: float32 [2048], P('fs'), may hold values from 0.1 to 1.9
- gate_weight: float32 [4, 2048, 1024], P(None, 'fs', 'tp'), may hold values from -0.125 to 0.125
- up_weight: float32 [4, 2048, 1024], P(None, 'fs', 'tp'), may hold values from -0.125 to 0.125
- down_weight: float32 [4, 2048, 1024], P(None, 'fs', 'tp'), may hold values from -0.5 to 0.5
- expert_ids: int32 [3072, 2], P(('grp', 'fs')), parts along dimension 0, may hold values from 0 to 3, as said below
- group_logits: float32 [3072, 2], P(('grp', 'fs')), parts along dimension 0, may hold values from -2.5 to 2.5
- pair_logits: float32 [3072, 2], P(('grp', 'fs')), parts along dimension 0, may hold values from -2.5 to 2.5
Outputs:
- mixed: bfloat16 [3072, 2048], P(('grp', 'fs'), 'tp'), parts along dimension 0
- gate_out: bfloat16 [8, 2048, 1024], P(('grp', 'fs'), None, 'tp'), parts along dimension 0
- up_out: bfloat16 [8, 2048, 1024], P(('grp', 'fs'), None, 'tp'), parts along dimension 0
- down_out: bfloat16 [8, 2048, 1024], P(('grp', 'fs'), None, 'tp'), parts along dimension 0
There are 2 independent parts, one for each index of `grp`. A program takes and returns all parts, laid end to end along the dimension named above; an argument that names none is the same for every part. Nothing has to cross between parts.
Inputs may be any that keep to these rules, and one draw needn't show every extreme that they name: `expert_ids`: each row names two different experts of one group: both ids lie in the same run of 2 consecutive ids.
All inputs are finite; a program needn't handle non-finite values.
Results may differ from a plain program's by a relative error of at most 0.015.
Values may be sent and summed in bfloat16 or wider, within the bound.
A program may use at most 64 MiB of HBM per device.

v0:
```python
import jax
import jax.numpy as jnp
from jax import lax
from jax.sharding import PartitionSpec as P


def routing(block_ids, experts, capacity):
    entries = block_ids.reshape(-1)
    onehot = (entries[:, None] == jnp.arange(experts, dtype=jnp.int32)[None, :]).astype(jnp.int32)
    before = jnp.cumsum(onehot, axis=0) - onehot
    entry_rank = jnp.sum(before * onehot, axis=1)
    kept = entry_rank < capacity
    slot_index = jnp.where(kept, entries * capacity + entry_rank, experts * capacity)
    return (slot_index, kept)


def fill_slots(block_rows, slot_index, experts, capacity):
    entry_count = slot_index.shape[0]
    source_row = jnp.arange(entry_count, dtype=jnp.int32) // 2
    slot_row = jnp.zeros((experts * capacity + 1,), jnp.int32).at[slot_index].set(source_row)
    filled = jnp.zeros((experts * capacity + 1,), jnp.float32).at[slot_index].set(1.0)
    chosen = block_rows[slot_row[: experts * capacity]]
    return chosen * filled[: experts * capacity, None].astype(block_rows.dtype)


def route_weights(block_ids, group_logits, pair_logits, kept, exp_group):
    group_pick = block_ids[:, 0] // exp_group
    group_exp = jnp.exp(group_logits)
    columns = jnp.arange(group_logits.shape[1], dtype=jnp.int32)
    chosen = jnp.sum(jnp.where(columns[None, :] == group_pick[:, None], group_exp, 0.0), axis=1)
    chosen = chosen / jnp.sum(group_exp, axis=1)
    pair_exp = jnp.exp(pair_logits)
    weights = pair_exp / jnp.sum(pair_exp, axis=1, keepdims=True) * chosen[:, None]
    return weights * kept.reshape(-1, 2).astype(weights.dtype)


def body(
    tokens, norm_gain, gate_weight, up_weight, down_weight, expert_ids, group_logits, pair_logits
):
    experts = gate_weight.shape[0]
    tok_rows = tokens.shape[0]
    capacity = 5 * tok_rows * 2 // (4 * experts)
    shard_count = lax.axis_size("fs")
    scaled = norm_gain[None, :, None]
    gate_cast = (scaled * gate_weight).astype(jnp.bfloat16)
    up_cast = (scaled * up_weight).astype(jnp.bfloat16)
    down_cast = down_weight.astype(jnp.bfloat16)
    slot_index, kept = routing(expert_ids, experts, capacity)
    weights = route_weights(
        expert_ids, group_logits, pair_logits, kept, experts // group_logits.shape[1]
    )
    gate_here, up_here, down_here = (
        lax.all_to_all(gate_cast, "fs", split_axis=0, concat_axis=1, tiled=True),
        lax.all_to_all(up_cast, "fs", split_axis=0, concat_axis=1, tiled=True),
        lax.all_to_all(down_cast, "fs", split_axis=0, concat_axis=1, tiled=True),
    )
    gate_local = gate_here[0]
    up_local = up_here[0]
    outgoing = fill_slots(tokens, slot_index, experts, capacity)
    arrived = lax.all_to_all(
        outgoing.reshape(experts, capacity, -1), "fs", split_axis=0, concat_axis=0, tiled=True
    )
    arrived = arrived.reshape(shard_count * capacity, -1)
    piece = lax.all_gather(arrived, "tp", axis=1, tiled=True)
    gate_pre = jnp.dot(piece, gate_local, preferred_element_type=jnp.float32)
    up_pre = jnp.dot(piece, up_local, preferred_element_type=jnp.float32)
    hidden = (jax.nn.silu(gate_pre) * up_pre).astype(jnp.bfloat16)
    terms = lax.dot_general(
        hidden, down_here[0], (((1,), (1,)), ((), ())), preferred_element_type=jnp.float32
    )
    expert_rows = lax.psum_scatter(
        terms.astype(jnp.bfloat16), "tp", scatter_dimension=1, tiled=True
    )
    returned = lax.all_to_all(
        expert_rows.reshape(shard_count, capacity, -1),
        "fs",
        split_axis=0,
        concat_axis=0,
        tiled=True,
    )
    returned = returned.reshape(experts * capacity, -1)
    picked = returned[jnp.clip(slot_index, 0, experts * capacity - 1)].astype(jnp.float32)
    picked = picked.reshape(tok_rows, 2, -1)
    mixed = jnp.sum(picked * weights[:, :, None], axis=1).astype(jnp.bfloat16)
    return (mixed, gate_here, up_here, down_here)


def solution(mesh):
    placed = (
        P(("grp", "fs"), "tp"),
        P("fs"),
        P(None, "fs", "tp"),
        P(None, "fs", "tp"),
        P(None, "fs", "tp"),
        P(("grp", "fs"), None),
        P(("grp", "fs"), None),
        P(("grp", "fs"), None),
    )
    return jax.shard_map(
        body,
        mesh=mesh,
        in_specs=placed,
        out_specs=(
            P(("grp", "fs"), "tp"),
            P(("grp", "fs"), None, "tp"),
            P(("grp", "fs"), None, "tp"),
            P(("grp", "fs"), None, "tp"),
        ),
        check_vma=False,
    )
```

profile of v0, /device:TPU:0, one launch (start us, length us, event | category | flops | bytes accessed | tf_op | source)
XLA Modules:
  0.0 240.4 jit_solution(12720926928837660163)
XLA Ops:
  7.2 0.0 copy-start
  7.2 0.0 all-gather.2.cloned.1.call-start
  7.2 0.9 copy.24
  8.1 0.1 eq.44
  8.2 0.1 eq.40
  8.4 0.7 broadcast_multiply_fusion.1
  9.1 1.1 reduce-window.6
  10.2 0.2 slice_reduce_fusion
  10.4 0.2 reduce-window.9
  10.6 0.1 add_bitcast_fusion
  10.7 0.1 copy.26
  10.9 0.2 mul.71
  11.1 3.4 %scatter_custom_fusion = s32[961]{0:T(1024)S(1)} fusion(s32[768]{0:T(1024)S(1)} %get-tuple-element.7, s32[768]{0:T(1024)S(1)} %add_select_fusion, s32[]{:T(128)} %constant.42.clone.1), kind=kCustom, calls=%fused_computation.53 | custom fusion | bytes 3848 | tf_op jit(solution)/shard_map/scatter | solution.py:20
  14.5 3.4 %scatter_custom_fusion.1 = f32[961]{0:T(1024)S(1)} fusion(s32[768]{0:T(1024)S(1)} %get-tuple-element.7, f32[768]{0:T(1024)S(1)} %broadcast.147, f32[]{:T(128)} %constant.49.clone.1), kind=kCustom, calls=%fused_computation.51 | custom fusion | bytes 3848 | tf_op jit(solution)/shard_map/scatter | solution.py:21
  17.9 0.1 convert_element_type.41
  18.0 0.0 copy-done
  18.0 4.1 %gather_fusion = bf16[960,512]{1,0:T(8,128)(2,1)S(1)} fusion(bf16[384,512]{1,0:T(8,128)(2,1)S(1)} %copy-done, s32[1024]{0:T(1024)S(1)} %pad_clamp_fusion.1), kind=kCustom, calls=%fused_computation | custom fusion | bytes 1969920 | tf_op jit(solution)/shard_map/gather | solution.py:22
  22.1 0.0 copy-start.3
  22.1 0.0 copy-start.7
  22.1 0.2 broadcast_multiply_fusion
  22.3 30.7 %all_to_all.46 = bf16[4,240,512]{2,1,0:T(8,128)(2,1)} all-to-all(bf16[4,240,512]{2,1,0:T(8,128)(2,1)S(1)} %broadcast_multiply_fusion), channel_id=1, replica_groups=mesh['grp'=2,'fs'=4,'tp'=4] {'fs'}, dimensions={0} | all-to-all | bytes 1966080 | tf_op jit(solution)/shard_map/all_to_all | solution.py:60
  53.0 0.0 all-gather.2.cloned.1.call-update
  53.0 0.0 copy-done.3
  53.0 0.0 copy-done.7
  53.0 2.9 %multiply_convert_fusion.1 = (bf16[4,512,256]{2,1,0:T(8,128)(2,1)S(1)}, bf16[4,512,256]{2,1,0:T(8,128)(2,1)}) fusion(f32[4,512,256]{2,1,0:T(8,128)S(1)} %copy-done.3, f32[512]{0:T(512)S(1)} %copy-done.7, f32[4,512,256]{2,1,0:T(8,128)} %param.11), kind=kLoop, calls=%fused_computation.6 | loop fusion | flops 2097152 | bytes 6293504 | tf_op jit(solution)/shard_map/convert_element_type | solution.py:45
  55.9 27.6 %all_to_all.47 = bf16[4,512,256]{2,1,0:T(8,128)(2,1)S(1)} all-to-all(bf16[4,512,256]{2,1,0:T(8,128)(2,1)S(1)} %get-tuple-element.8), channel_id=1, replica_groups=mesh['grp'=2,'fs'=4,'tp'=4] {'fs'}, dimensions={0} | all-to-all | bytes 2097152 | tf_op jit(solution)/shard_map/all_to_all | solution.py:53
  83.5 3.5 %all-to-all-start.2 = ((bf16[4,512,256]{2,1,0:T(8,128)(2,1)}), bf16[4,512,256]{2,1,0:T(8,128)(2,1)S(1)}, u32[]{:S(2)}, u32[]{:S(2)}) async-start(bf16[4,512,256]{2,1,0:T(8,128)(2,1)} %get-tuple-element.9), calls=%async_computation.2 | async-start | bytes 2097152 | tf_op jit(solution)/shard_map/all_to_all | solution.py:54
  87.1 2.7 %convert_element_type.45 = bf16[4,512,256]{2,1,0:T(8,128)(2,1)} convert(f32[4,512,256]{2,1,0:T(8,128)} %param.12) | non-fusion elementwise | flops 524288 | bytes 3145728 | tf_op jit(solution)/shard_map/convert_element_type | solution.py:47
  89.7 22.1 %all-to-all-done.2 = bf16[4,512,256]{2,1,0:T(8,128)(2,1)S(1)} async-done(((bf16[4,512,256]{2,1,0:T(8,128)(2,1)}), bf16[4,512,256]{2,1,0:T(8,128)(2,1)S(1)}, u32[]{:S(2)}, u32[]{:S(2)}) %all-to-all-start.2) | async-done | bytes 1048608 | tf_op jit(solution)/shard_map/all_to_all | solution.py:54
  111.8 0.0 copy-start.1
  111.8 4.2 %all-to-all-start.3 = ((bf16[4,512,256]{2,1,0:T(8,128)(2,1)}), bf16[4,512,256]{2,1,0:T(8,128)(2,1)}, u32[]{:S(2)}, u32[]{:S(2)}) async-start(bf16[4,512,256]{2,1,0:T(8,128)(2,1)} %convert_element_type.45), calls=%async_computation.3 | async-start | bytes 2097152 | tf_op jit(solution)/shard_map/all_to_all | solution.py:55
  116.1 0.0 reduce-scatter.2.cloned.1.call-start
  116.1 0.0 all-gather.2.cloned.1.call-done
  116.2 3.3 %fusion.23 = f32[960,256]{1,0:T(8,128)S(1)} fusion(bf16[960,2048]{1,0:T(8,128)(2,1)} %all-gather.2.cloned.1.call-done, bf16[2048,256]{1,0:T(8,128)(2,1)S(1)} %bitcast.36), kind=kOutput, calls=%fused_computation.58 | convolution fusion | flops 1006632960 | bytes 5963776 | tf_op jit(solution)/shard_map/dot_general | solution.py:65
  119.5 22.0 %all-to-all-done.3 = bf16[4,512,256]{2,1,0:T(8,128)(2,1)} async-done(((bf16[4,512,256]{2,1,0:T(8,128)(2,1)}), bf16[4,512,256]{2,1,0:T(8,128)(2,1)}, u32[]{:S(2)}, u32[]{:S(2)}) %all-to-all-start.3) | async-done | bytes 1048608 | tf_op jit(solution)/shard_map/all_to_all | solution.py:55
  141.4 0.0 copy-done.1
  141.4 8.4 %convolution_convert_fusion = bf16[960,2048]{1,0:T(8,128)(2,1)} fusion(bf16[2048,256]{1,0:T(8,128)(2,1)} %bitcast.5, bf16[960,2048]{1,0:T(8,128)(2,1)} %all-gather.2.cloned.1.call-done, bf16[2048,256]{1,0:T(8,128)(2,1)S(1)} %bitcast.38, f32[960,256]{1,0:T(8,128)S(1)} %fusion.23), kind=kOutput, calls=%fused_computation.4 | convolution fusion | flops 2016706560 | bytes 10944512 | tf_op jit(solution)/shard_map/dot_general | solution.py:68
  149.8 0.0 copy-start.4
  149.8 0.0 copy-start.6
  149.8 0.0 copy-start.5
  149.8 0.0 reduce-scatter.2.cloned.1.call-update
  149.9 42.0 %reduce-scatter.2.cloned.1.call-done = bf16[960,512]{1,0:T(8,128)(2,1)} async-done(((bf16[960,2048]{1,0:T(8,128)(2,1)}), bf16[960,512]{1,0:T(8,128)(2,1)}) %reduce-scatter.2.cloned.1.call-update) | async-done | bytes 983056 | tf_op jit(solution)/shard_map/reduce_scatter | solution.py:71
  191.9 4.6 %all-to-all-start.4 = ((bf16[4,240,512]{2,1,0:T(8,128)(2,1)}), bf16[4,240,512]{2,1,0:T(8,128)(2,1)S(1)}, u32[]{:S(2)}, u32[]{:S(2)}) async-start(bf16[4,240,512]{2,1,0:T(8,128)(2,1)} %bitcast.42), calls=%async_computation.5 | async-start | bytes 1966080 | tf_op jit(solution)/shard_map/all_to_all | solution.py:74
  196.5 0.2 lt.53
  196.7 0.1 copy.27
  196.8 0.0 copy-done.4
  196.8 0.0 copy-done.6
  196.9 0.0 copy-done.5
  196.9 0.1 copy.28
  197.1 23.5 %all-to-all-done.4 = bf16[4,240,512]{2,1,0:T(8,128)(2,1)S(1)} async-done(((bf16[4,240,512]{2,1,0:T(8,128)(2,1)}), bf16[4,240,512]{2,1,0:T(8,128)(2,1)S(1)}, u32[]{:S(2)}, u32[]{:S(2)}) %all-to-all-start.4) | async-done | bytes 983072 | tf_op jit(solution)/shard_map/all_to_all | solution.py:74
  220.6 3.3 %gather_fusion.1 = bf16[768,512]{1,0:T(8,128)(2,1)} fusion(bf16[960,512]{1,0:T(8,128)(2,1)S(1)} %bitcast.35, s32[1024]{0:T(1024)S(1)} %pad_clamp_fusion), kind=kCustom, calls=%fused_computation.1 | custom fusion | bytes 1575936 | tf_op jit(solution)/shard_map/gather | solution.py:82
  223.9 2.1 reshape.135
  226.1 0.0 copy-start.2
  226.1 3.2 %multiply_reduce_fusion = bf16[384,512]{1,0:T(8,128)(2,1)} fusion(f32[384,2,512]{2,1,0:T(2,128)S(1)} %reshape.135, f32[384,2]{1,0:T(8,128)S(1)} %copy.28), kind=kLoop, calls=%fused_computation.7 | loop fusion | flops 589824 | bytes 1969152 | tf_op jit(solution)/shard_map/reduce_sum | solution.py:84
  229.3 1.0 copy.34
  230.3 0.0 copy-done.2
  230.3 1.0 copy.35
  231.3 2.3 copy.36
  (15 shorter events, 0.2 us)
Async XLA Ops:
  7.2 10.8 %copy-start = (bf16[384,512]{1,0:T(8,128)(2,1)S(1)}, bf16[384,512]{1,0:T(8,128)(2,1)}, u32[]{:S(2)}) copy-start(bf16[384,512]{1,0:T(8,128)(2,1)} %param.8) | copy-start | bytes 1179652
  7.2 109.0 %all-gather.2.cloned.1.call-start = ((), (), s32[]{:S(2)}) async-start(), calls=%async_computation.6 | async-start | bytes 4915200 | tf_op jit(solution)/shard_map/all_gather | solution.py:64
  22.1 31.0 %copy-start.3 = (f32[4,512,256]{2,1,0:T(8,128)S(1)}, f32[4,512,256]{2,1,0:T(8,128)}, u32[]{:S(2)}) copy-start(f32[4,512,256]{2,1,0:T(8,128)} %param.10) | copy-start | bytes 6291460
  22.1 31.0 %copy-start.7 = (f32[512]{0:T(512)S(1)}, f32[512]{0:T(512)}, u32[]{:S(2)}) copy-start(f32[512]{0:T(512)} %param.9) | copy-start | bytes 6148
  83.5 28.3 %all-to-all-start.2 = ((bf16[4,512,256]{2,1,0:T(8,128)(2,1)}), bf16[4,512,256]{2,1,0:T(8,128)(2,1)S(1)}, u32[]{:S(2)}, u32[]{:S(2)}) async-start(bf16[4,512,256]{2,1,0:T(8,128)(2,1)} %get-tuple-element.9), calls=%async_computation.2 | async-start | bytes 2097152 | tf_op jit(solution)/shard_map/all_to_all | solution.py:54
  111.8 29.6 %copy-start.1 = (bf16[4,512,256]{2,1,0:T(8,128)(2,1)}, bf16[4,512,256]{2,1,0:T(8,128)(2,1)S(1)}, u32[]{:S(2)}) copy-start(bf16[4,512,256]{2,1,0:T(8,128)(2,1)S(1)} %all-to-all-done.2) | copy-start | bytes 3145732
  111.8 29.6 %all-to-all-start.3 = ((bf16[4,512,256]{2,1,0:T(8,128)(2,1)}), bf16[4,512,256]{2,1,0:T(8,128)(2,1)}, u32[]{:S(2)}, u32[]{:S(2)}) async-start(bf16[4,512,256]{2,1,0:T(8,128)(2,1)} %convert_element_type.45), calls=%async_computation.3 | async-start | bytes 2097152 | tf_op jit(solution)/shard_map/all_to_all | solution.py:55
  116.1 75.8 %reduce-scatter.2.cloned.1.call-start = ((), (), s32[]{:S(2)}) async-start(), calls=%async_computation.7 | async-start | bytes 4915200 | tf_op jit(solution)/shard_map/reduce_scatter | solution.py:71
  149.8 47.0 %copy-start.4 = (s32[384,2]{0,1:T(2,128)S(1)}, s32[384,2]{0,1:T(2,128)}, u32[]{:S(2)}) copy-start(s32[384,2]{0,1:T(2,128)} %param.13) | copy-start | bytes 9220
  149.8 47.0 %copy-start.6 = (f32[384,2]{0,1:T(2,128)S(1)}, f32[384,2]{0,1:T(2,128)}, u32[]{:S(2)}) copy-start(f32[384,2]{0,1:T(2,128)} %param.14) | copy-start | bytes 9220
  149.8 47.1 %copy-start.5 = (f32[384,2]{0,1:T(2,128)S(1)}, f32[384,2]{0,1:T(2,128)}, u32[]{:S(2)}) copy-start(f32[384,2]{0,1:T(2,128)} %param.15) | copy-start | bytes 9220
  191.9 28.7 %all-to-all-start.4 = ((bf16[4,240,512]{2,1,0:T(8,128)(2,1)}), bf16[4,240,512]{2,1,0:T(8,128)(2,1)S(1)}, u32[]{:S(2)}, u32[]{:S(2)}) async-start(bf16[4,240,512]{2,1,0:T(8,128)(2,1)} %bitcast.42), calls=%async_computation.5 | async-start | bytes 1966080 | tf_op jit(solution)/shard_map/all_to_all | solution.py:74
  226.1 4.2 %copy-start.2 = (bf16[4,512,256]{2,1,0:T(8,128)(2,1)S(1)}, bf16[4,512,256]{2,1,0:T(8,128)(2,1)}, u32[]{:S(2)}) copy-start(bf16[4,512,256]{2,1,0:T(8,128)(2,1)} %copy-done.1) | copy-start | bytes 3145732
Sparse Core Ops, SparseCore 0:
  53.1 32.0 all-gather.1
  150.0 41.8 reduce-scatter.1
where the time goes:
time: 241 us; the launch traced here: 240 us
  waiting for transfers between devices  110 us (46%)
  blocking collectives  58.3 us (24%)
  local copies, waits for them, and re-layouts  22.7 us (9%)
  between operations  14.3 us (6%)
  starting transfers between devices  12.4 us (5%)
  matrix products  11.7 us (5%)
  other arithmetic  11.2 us (5%)
    reduce_scatter x1, waiting for transfers between devices, body(): lax.psum_scatter(terms.astype(jnp.bfloat16), 'tp', scatter_dimension=1, t...  42 us
    all_to_all x1, blocking collectives, body(): lax.all_to_all(outgoing.reshape(experts, capacity, -1), 'fs', split_axis=...  30.7 us
    all_to_all x1, blocking collectives, body(): lax.all_to_all(gate_cast, 'fs', split_axis=0, concat_axis=1, tiled=True)  27.6 us
    all_to_all x1, waiting for transfers between devices, body(): lax.all_to_all(expert_rows.reshape(shard_count, capacity, -1), 'fs', spli...  23.5 us
    all_to_all x1, waiting for transfers between devices, body(): lax.all_to_all(up_cast, 'fs', split_axis=0, concat_axis=1, tiled=True)  22.1 us
    all_to_all x1, waiting for transfers between devices, body(): lax.all_to_all(down_cast, 'fs', split_axis=0, concat_axis=1, tiled=True)  22 us
    dot_general x1, matrix products, body(): lax.dot_general(hidden, down_here[0], (((1,), (1,)), ((), ())), preferred...  8.4 us
    unnamed x20, local copies, waits for them, and re-layouts  5.1 us
  transfers between devices with their start and end apart: 5, of which 4 were waited for; matrix products, arithmetic and copies ran while one was open for 4% of the time, Pallas kernels for 0%

commit v1 on v0

v1 whole, which is shorter than its diff:
```python
import functools

import jax
import jax.numpy as jnp
from jax import lax
from jax.experimental import pallas as pl
from jax.experimental.pallas import tpu as pltpu
from jax.sharding import PartitionSpec as P

MESH = pl.DeviceIdType.MESH
BF16 = jnp.bfloat16
F32 = jnp.float32


def each(count, step):
    if count <= 4:
        for i in range(count):
            step(i)
    else:
        lax.fori_loop(0, count, lambda i, c: (step(i), c)[1], 0)


def exchange_kernel(
    n_grp, n_fs, n_tp,
    out_ref, gate_in, up_in, down_in,
    ret, gate_out, up_out, down_out,
    piece, hidden, own, pair_send, pair_recv, x_send, x_recv, result,
    local_sem, slot_s, slot_r, wz_s, wz_r, wy_s, wy_r,
    gx_s, gx_r, gd_s, gd_r, gf_s, gf_r, pr_s, pr_r, xx_s, xx_r, rt_s, rt_r,
):
    g, f, t = lax.axis_index("grp"), lax.axis_index("fs"), lax.axis_index("tp")
    n_x = n_tp // 2
    chip, core = t // 2, lax.rem(t, 2)
    partner = chip * 2 + 1 - core
    width = piece.shape[3]
    block = gate_in.shape[1]
    share = block // n_grp

    def fs_at(k):
        return lax.rem(f + k, n_fs)

    def grp_at(k):
        return lax.rem(g + k, n_grp)

    def chip_at(k):
        return lax.rem(chip + k, n_x)

    def rcopy(src, dst, ssem, rsem, axis, peer):
        return pltpu.make_async_remote_copy(
            src_ref=src, dst_ref=dst, send_sem=ssem, recv_sem=rsem,
            device_id={axis: peer}, device_id_type=MESH,
        )

    barrier = pltpu.get_barrier_semaphore()

    def greet(axis, peer):
        pl.semaphore_signal(barrier, inc=1, device_id={axis: peer}, device_id_type=MESH)

    each(n_fs - 1, lambda i: greet("fs", fs_at(i + 1)))
    each(n_grp - 1, lambda i: greet("grp", grp_at(i + 1)))
    each(n_x - 1, lambda i: greet("tp", chip_at(i + 1) * 2 + core))
    greet("tp", partner)
    pl.semaphore_wait(barrier, n_fs - 1 + n_grp - 1 + n_x - 1 + 1)

    weights = ((gate_in, gate_out), (up_in, up_out), (down_in, down_out))

    def slot_copy(k, source):
        return rcopy(out_ref.at[fs_at(k)], piece.at[t, source], slot_s.at[k],
                     slot_r.at[n_fs - k], "fs", fs_at(k))

    def slot_arrival(k):
        return rcopy(out_ref.at[f], piece.at[t, fs_at(k)], slot_s.at[k], slot_r.at[k], "fs", fs_at(k))

    each(n_fs - 1, lambda i: slot_copy(i + 1, f).start())
    own_slots = pltpu.make_async_copy(out_ref.at[f], piece.at[t, f], local_sem.at[3])
    own_slots.start()

    def w_rows(source, part):
        return pl.ds(source * block + part * share, share)

    def wz_copy(m, k):
        w_in, w_out = weights[m]
        return rcopy(w_in.at[fs_at(k), pl.ds(g * share, share)], w_out.at[w_rows(f, g)],
                     wz_s.at[m, k], wz_r.at[m, n_fs - k], "fs", fs_at(k))

    def wz_arrival(m, k):
        w_in, w_out = weights[m]
        return rcopy(w_in.at[fs_at(k), pl.ds(g * share, share)], w_out.at[w_rows(fs_at(k), g)],
                     wz_s.at[m, k], wz_r.at[m, k], "fs", fs_at(k))

    def wy_copy(m, k, j):
        w_out = weights[m][1]
        rows = w_rows(fs_at(k), g)
        return rcopy(w_out.at[rows], w_out.at[rows], wy_s.at[m, k, j],
                     wy_r.at[m, k, n_grp - j], "grp", grp_at(j))

    def wy_arrival(m, k, j):
        w_out = weights[m][1]
        rows = w_rows(fs_at(k), grp_at(j))
        return rcopy(w_out.at[rows], w_out.at[rows], wy_s.at[m, k, j],
                     wy_r.at[m, k, j], "grp", grp_at(j))

    own_weights = []
    for m in range(3):
        w_in, w_out = weights[m]
        each(n_fs - 1, lambda i: wz_copy(m, i + 1).start())
        copy = pltpu.make_async_copy(w_in.at[f], w_out.at[pl.ds(f * block, block)], local_sem.at[m])
        copy.start()
        own_weights.append(copy)

    def forward(m, k):
        wz_arrival(m, k).wait_recv()
        for j in range(1, n_grp):
            wy_copy(m, k, j).start()

    def gx_copy(k, j):
        src = piece.at[t, fs_at(k)]
        return rcopy(src, src, gx_s.at[k, j], gx_r.at[k, n_x - j], "tp", chip_at(j) * 2 + core)

    def gx_arrival(k, j):
        src = piece.at[chip_at(j) * 2 + core, fs_at(k)]
        return rcopy(src, src, gx_s.at[k, j], gx_r.at[k, j], "tp", chip_at(j) * 2 + core)

    def gd_copy(k):
        src = piece.at[t, fs_at(k)]
        return rcopy(src, src, gd_s.at[k], gd_r.at[k], "tp", partner)

    def gd_arrival(k):
        src = piece.at[partner, fs_at(k)]
        return rcopy(src, src, gd_s.at[k], gd_r.at[k], "tp", partner)

    def gf_copy(k, j):
        src = piece.at[chip_at(j) * 2 + core, fs_at(k)]
        return rcopy(src, src, gf_s.at[k, j], gf_r.at[k, j], "tp", partner)

    def gf_arrival(k, j):
        src = piece.at[chip_at(j) * 2 + 1 - core, fs_at(k)]
        return rcopy(src, src, gf_s.at[k, j], gf_r.at[k, j], "tp", partner)

    def spread(k):
        for j in range(1, n_x):
            gx_copy(k, j).start()
        gd_copy(k).start()

    own_slots.wait()
    spread(0)

    def spread_arrived(i):
        slot_arrival(i + 1).wait_recv()
        spread(i + 1)

    each(n_fs - 1, spread_arrived)

    def hand_over(k):
        for j in range(1, n_x):
            gx_arrival(k, j).wait_recv()
            gf_copy(k, j).start()

    hand_over(0)

    def hand_and_forward(i):
        hand_over(i + 1)
        forward(0, i + 1)

    each(n_fs - 1, hand_and_forward)
    each(n_fs - 1, lambda i: forward(1, i + 1))

    def all_in(m):
        own_weights[m].wait()
        for j in range(1, n_grp):
            each(n_fs - 1, lambda i: wy_arrival(m, i + 1, j).wait_recv())

    all_in(0)
    all_in(1)

    def make_hidden(k):
        source = fs_at(k)
        gd_arrival(k).wait_recv()
        for j in range(1, n_x):
            gf_arrival(k, j).wait_recv()
        gate = up = None
        for p in range(n_tp):
            rows = piece[p, source]
            cols = pl.ds(p * width, width)
            gate_part = jnp.dot(rows, gate_out[cols, :], preferred_element_type=F32)
            up_part = jnp.dot(rows, up_out[cols, :], preferred_element_type=F32)
            gate = gate_part if gate is None else gate + gate_part
            up = up_part if up is None else up + up_part
        hidden[k] = (gate / (1.0 + jnp.exp(-gate)) * up).astype(BF16)

    def hidden_and_forward(i):
        make_hidden(i + 1)
        forward(2, i + 1)

    each(n_fs - 1, hidden_and_forward)
    make_hidden(0)
    all_in(2)

    def term(k, j, to_core):
        column = (chip_at(j) * 2 + to_core) * width
        rows = down_out[pl.ds(pl.multiple_of(column, width), width), :]
        return lax.dot_general(hidden[k], rows, (((1,), (1,)), ((), ())), preferred_element_type=F32)

    def pr_copy(k):
        return rcopy(pair_send.at[k], pair_recv.at[k], pr_s.at[k], pr_r.at[k], "tp", partner)

    def stage_pair(k):
        for j in range(n_x):
            pair_send[k, j] = term(k, j, 1 - core).astype(BF16)
        pr_copy(k).start()
        for j in range(n_x):
            own[k, j] = term(k, j, core)

    def xx_copy(k, j):
        return rcopy(x_send.at[k, j], x_recv.at[k, n_x - j], xx_s.at[k, j], xx_r.at[k, n_x - j],
                     "tp", chip_at(j) * 2 + core)

    def xx_arrival(k, j):
        return rcopy(x_send.at[k, j], x_recv.at[k, j], xx_s.at[k, j], xx_r.at[k, j],
                     "tp", chip_at(j) * 2 + core)

    def stage_chip(k):
        pr_copy(k).wait_recv()
        for j in range(1, n_x):
            x_send[k, j] = (own[k, j] + pair_recv[k, j].astype(F32)).astype(BF16)
            xx_copy(k, j).start()
        own[k, 0] = own[k, 0] + pair_recv[k, 0].astype(F32)

    def rt_copy(k):
        return rcopy(result.at[k], ret.at[f], rt_s.at[k], rt_r.at[n_fs - k], "fs", fs_at(k))

    def rt_arrival(k):
        return rcopy(result.at[k], ret.at[fs_at(k)], rt_s.at[k], rt_r.at[k], "fs", fs_at(k))

    def total(k):
        acc = own[k, 0]
        for j in range(1, n_x):
            xx_arrival(k, j).wait_recv()
            acc = acc + x_recv[k, j].astype(F32)
        return acc.astype(BF16)

    def stage_home(k):
        result[k] = total(k)
        rt_copy(k).start()

    def order(i):
        return i + 1 if n_fs <= 4 and i + 1 < n_fs else lax.rem(i + 1, n_fs)

    stage_pair(order(0))

    def pair_and_chip(i):
        stage_pair(order(i + 1))
        stage_chip(order(i))

    each(n_fs - 1, pair_and_chip)
    stage_chip(order(n_fs - 1))
    each(n_fs - 1, lambda i: stage_home(i + 1))
    ret[f] = total(0)
    each(n_fs - 1, lambda i: rt_arrival(i + 1).wait_recv())

    def drain_peer(i):
        k = i + 1
        slot_copy(k, f).wait_send()
        rt_copy(k).wait_send()
        for m in range(3):
            wz_copy(m, k).wait_send()
            for j in range(1, n_grp):
                wy_copy(m, k, j).wait_send()

    def drain_chunk(k):
        gd_copy(k).wait_send()
        pr_copy(k).wait_send()
        for j in range(1, n_x):
            gx_copy(k, j).wait_send()
            gf_copy(k, j).wait_send()
            xx_copy(k, j).wait_send()

    each(n_fs - 1, drain_peer)
    each(n_fs, drain_chunk)


def exchange(n_grp, n_fs, n_tp, outgoing, gate, up, down):
    n_x = n_tp // 2
    cap, width = outgoing.shape[1:]
    block, hid = gate.shape[1:]
    vmem = pl.BlockSpec(memory_space=pltpu.VMEM)
    dma = pltpu.SemaphoreType.DMA
    matrix = jax.ShapeDtypeStruct((n_fs * block, hid), BF16)
    chunk = (n_fs, n_x, cap, width)
    sem_shapes = [
        (4,), (n_fs,), (n_fs,), (3, n_fs), (3, n_fs), (3, n_fs, n_grp), (3, n_fs, n_grp),
        (n_fs, n_x), (n_fs, n_x), (n_fs,), (n_fs,), (n_fs, n_x), (n_fs, n_x),
        (n_fs,), (n_fs,), (n_fs, n_x), (n_fs, n_x), (n_fs,), (n_fs,),
    ]
    return pl.pallas_call(
        functools.partial(exchange_kernel, n_grp, n_fs, n_tp),
        out_shape=(jax.ShapeDtypeStruct((n_fs, cap, width), BF16), matrix, matrix, matrix),
        in_specs=[vmem] * 4,
        out_specs=(vmem,) * 4,
        scratch_shapes=[
            pltpu.VMEM((n_tp, n_fs, cap, width), BF16),
            pltpu.VMEM((n_fs, cap, hid), BF16),
            pltpu.VMEM(chunk, F32),
            pltpu.VMEM(chunk, BF16),
            pltpu.VMEM(chunk, BF16),
            pltpu.VMEM(chunk, BF16),
            pltpu.VMEM(chunk, BF16),
            pltpu.VMEM((n_fs, cap, width), BF16),
        ] + [dma(s) for s in sem_shapes],
        compiler_params=pltpu.CompilerParams(
            collective_id=0, has_side_effects=True, vmem_limit_bytes=56 * 1024 * 1024
        ),
    )(outgoing, gate, up, down)


def body(
    tokens, norm_gain, gate_weight, up_weight, down_weight, expert_ids, group_logits, pair_logits
):
    n_grp, n_fs, n_tp = (lax.axis_size(a) for a in ("grp", "fs", "tp"))
    experts = gate_weight.shape[0]
    tok_rows = tokens.shape[0]
    capacity = 5 * tok_rows * 2 // (4 * experts)
    padded = -(-capacity // 16) * 16
    slots = experts * padded

    columns = jnp.arange(experts, dtype=jnp.int32)
    named = [(expert_ids[:, k, None] == columns[None, :]).astype(F32) for k in range(2)]
    rows = jnp.arange(tok_rows, dtype=jnp.int32)
    earlier = (rows[None, :] < rows[:, None]).astype(BF16)
    before = jnp.dot(earlier, (named[0] + named[1]).astype(BF16), preferred_element_type=F32)
    picks, kept = [], []
    for k in range(2):
        rank = jnp.sum(before * named[k], axis=1).astype(jnp.int32)
        kept.append(rank < capacity)
        picks.append(jnp.where(kept[k], expert_ids[:, k] * padded + rank, slots))
    slot_ids = jnp.arange(slots, dtype=jnp.int32)
    place = [(picks[k][:, None] == slot_ids[None, :]).astype(BF16) for k in range(2)]
    outgoing = lax.dot_general(
        place[0] + place[1], tokens, (((0,), (0,)), ((), ())), preferred_element_type=F32
    ).astype(BF16).reshape(experts, padded, -1)

    scaled = norm_gain[None, :, None]
    gate_cast = (scaled * gate_weight).astype(BF16)
    up_cast = (scaled * up_weight).astype(BF16)
    down_cast = down_weight.astype(BF16)
    returned, gate_here, up_here, down_here = exchange(
        n_grp, n_fs, n_tp, outgoing, gate_cast, up_cast, down_cast
    )
    returned = returned.reshape(slots, -1)

    group_exp = jnp.exp(group_logits)
    group_count = group_logits.shape[1]
    group_pick = expert_ids[:, 0] // (experts // group_count)
    groups = jnp.arange(group_count, dtype=jnp.int32)
    chosen = jnp.sum(jnp.where(groups[None, :] == group_pick[:, None], group_exp, 0.0), axis=1)
    chosen = chosen / jnp.sum(group_exp, axis=1)
    pair_exp = jnp.exp(pair_logits)
    weights = pair_exp / jnp.sum(pair_exp, axis=1, keepdims=True) * chosen[:, None]
    mixed = 0.0
    for k in range(2):
        weight = weights[:, k] * kept[k].astype(F32)
        picked = jnp.dot(place[k], returned, preferred_element_type=F32)
        mixed = mixed + picked * weight[:, None]
    return (mixed.astype(BF16), gate_here[None], up_here[None], down_here[None])


def solution(mesh):
    placed = (
        P(("grp", "fs"), "tp"),
        P("fs"),
        P(None, "fs", "tp"),
        P(None, "fs", "tp"),
        P(None, "fs", "tp"),
        P(("grp", "fs"), None),
        P(("grp", "fs"), None),
        P(("grp", "fs"), None),
    )
    return jax.shard_map(
        body,
        mesh=mesh,
        in_specs=placed,
        out_specs=(
            P(("grp", "fs"), "tp"),
            P(("grp", "fs"), None, "tp"),
            P(("grp", "fs"), None, "tp"),
            P(("grp", "fs"), None, "tp"),
        ),
        check_vma=False,
    )
```

time: 241 us -> 133 us (0.55)
  the two profiles are of different devices: /device:TPU:0 before, /device:TPU:29 now
where the time goes in v1:
time: 133 us; the launch traced here: 132 us
  Pallas kernels  113 us (85%)
  other arithmetic  7.43 us (6%)
  local copies, waits for them, and re-layouts  5.87 us (4%)
  matrix products  5.34 us (4%)
    pallas_call x1, Pallas kernels, exchange(): pl.pallas_call(functools.partial(exchange_kernel, n_grp, n_fs, n_tp), out...  113 us
    unnamed x19, local copies, waits for them, and re-layouts  5.1 us
    convert_element_type x1, other arithmetic, body(): up_cast = (scaled * up_weight).astype(BF16)  3.28 us
    dot_general x2, matrix products, body(): picked = jnp.dot(place[k], returned, preferred_element_type=F32)  3.27 us

profile of v1, /device:TPU:29, one launch (start us, length us, event | category | flops | bytes accessed | tf_op | source)
XLA Modules:
  0.0 132.3 jit_solution(12351607198501085953)
XLA Ops:
  0.6 0.0 copy-start
  0.6 0.8 exponential_reduce_fusion.1
  1.4 0.8 slice_reduce_fusion.1
  2.2 0.2 select_reduce_fusion.1
  2.4 0.0 copy-start.1
  2.4 0.9 fusion.23
  3.3 0.7 exponential_reduce_fusion
  4.0 0.7 divide_multiply_fusion
  4.7 0.0 copy-done
  4.8 1.9 %convolution_convert_fusion = bf16[960,512]{1,0:T(8,128)(2,1)} fusion(bf16[384,512]{1,0:T(8,128)(2,1)S(1)} %copy-done, s32[384]{0:T(512)S(1)} %get-tuple-element.20, s32[384]{0:T(512)S(1)} %get-tuple-element.19), kind=kOutput, calls=%fused_computation.8 | convolution fusion | flops 380928000 | bytes 1379328 | tf_op jit(solution)/shard_map/dot_general | solution.py:338
  6.6 0.0 copy-done.1
  6.6 0.0 copy-start.2
  6.6 0.0 copy-start.6
  6.6 1.1 convert_element_type.79.down_in
  7.7 0.9 copy-done.2
  8.6 0.0 copy-done.6
  8.6 3.3 %multiply_convert_fusion = (bf16[4,512,256]{2,1,0:T(8,128)(2,1)}, bf16[4,512,256]{2,1,0:T(8,128)(2,1)}) fusion(f32[4,512,256]{2,1,0:T(8,128)S(1)} %copy-done.2, f32[512]{0:T(512)S(1)} %copy-done.6, f32[4,512,256]{2,1,0:T(8,128)} %param.10), kind=kLoop, calls=%fused_computation | loop fusion | flops 2097152 | bytes 6293504 | tf_op jit(solution)/shard_map/convert_element_type | solution.py:344
  11.9 112.9 %shard_map.111 = (bf16[4,240,512]{2,1,0:T(8,128)(2,1)}, bf16[2048,256]{1,0:T(8,128)(2,1)}, bf16[2048,256]{1,0:T(8,128)(2,1)}, bf16[2048,256]{1,0:T(8,128)(2,1)}) custom-call(bf16[4,240,512]{2,1,0:T(8,128)(2,1)} %bitcast.11, bf16[4,512,256]{2,1,0:T(8,128)(2,1)} %get-tuple-element.24.gate_in, bf16[4,512,256]{2,1,0:T(8,128)(2,1)} %get-tuple-element.23.up_in, ...), custom_call_target="tpu_custom_call" | custom-call | tf_op jit(solution)/shard_map/pallas_call | solution.py:295
  124.8 0.0 copy-start.7
  124.8 1.9 %fusion.6 = f32[384,512]{1,0:T(8,128)S(1)} fusion(bf16[960,512]{1,0:T(8,128)(2,1)} %bitcast.12, s32[384]{0:T(512)S(1)} %get-tuple-element.20, f32[384]{0:T(512)S(1)} %get-tuple-element.15), kind=kOutput, calls=%fused_computation.11 | convolution fusion | flops 378052608 | bytes 1772544 | tf_op jit(solution)/shard_map/dot_general | solution.py:362
  126.7 0.0 copy-done.7
  126.7 0.0 copy-start.5
  126.7 1.4 %fusion.7 = bf16[384,512]{1,0:T(8,128)(2,1)} fusion(f32[384,512]{1,0:T(8,128)S(1)} %fusion.6, bf16[960,512]{1,0:T(8,128)(2,1)S(1)} %bitcast.13, s32[384]{0:T(512)S(1)} %get-tuple-element.19, f32[384]{0:T(512)S(1)} %get-tuple-element.14), kind=kOutput, calls=%fused_computation.12 | convolution fusion | flops 378445824 | bytes 2165760 | tf_op jit(solution)/shard_map/dot_general | solution.py:362
  128.1 0.0 copy-done.5
  128.1 0.0 copy-start.4
  128.1 1.0 copy.15
  129.1 0.6 copy-done.4
  129.7 0.0 copy-start.3
  129.7 1.0 copy.16
  130.7 0.6 copy-done.3
  131.3 1.0 copy.17
  (4 shorter events, 0.0 us)
Async XLA Ops:
  0.6 4.1 %copy-start = (bf16[384,512]{1,0:T(8,128)(2,1)S(1)}, bf16[384,512]{1,0:T(8,128)(2,1)}, u32[]{:S(2)}) copy-start(bf16[384,512]{1,0:T(8,128)(2,1)} %param.8) | copy-start | bytes 1179652
  2.4 4.2 %copy-start.1 = (f32[4,512,256]{2,1,0:T(8,128)S(1)}, f32[4,512,256]{2,1,0:T(8,128)}, u32[]{:S(2)}) copy-start(f32[4,512,256]{2,1,0:T(8,128)} %param.12) | copy-start | bytes 6291460
  6.6 2.0 %copy-start.2 = (f32[4,512,256]{2,1,0:T(8,128)S(1)}, f32[4,512,256]{2,1,0:T(8,128)}, u32[]{:S(2)}) copy-start(f32[4,512,256]{2,1,0:T(8,128)} %param.11) | copy-start | bytes 6291460
  6.6 2.0 %copy-start.6 = (f32[512]{0:T(512)S(1)}, f32[512]{0:T(512)}, u32[]{:S(2)}) copy-start(f32[512]{0:T(512)} %param.9) | copy-start | bytes 6148
  124.8 1.9 %copy-start.7 = (bf16[4,240,512]{2,1,0:T(8,128)(2,1)S(1)}, bf16[4,240,512]{2,1,0:T(8,128)(2,1)}, u32[]{:S(2)}) copy-start(bf16[4,240,512]{2,1,0:T(8,128)(2,1)} %get-tuple-element.8) | copy-start | bytes 2949124
  126.7 1.4 %copy-start.5 = (bf16[2048,256]{1,0:T(8,128)(2,1)S(1)}, bf16[2048,256]{1,0:T(8,128)(2,1)}, u32[]{:S(2)}) copy-start(bf16[2048,256]{1,0:T(8,128)(2,1)} %get-tuple-element.9) | copy-start | bytes 3145732
  128.1 1.6 %copy-start.4 = (bf16[2048,256]{1,0:T(8,128)(2,1)S(1)}, bf16[2048,256]{1,0:T(8,128)(2,1)}, u32[]{:S(2)}) copy-start(bf16[2048,256]{1,0:T(8,128)(2,1)} %get-tuple-element.10) | copy-start | bytes 3145732
  129.7 1.6 %copy-start.3 = (bf16[2048,256]{1,0:T(8,128)(2,1)S(1)}, bf16[2048,256]{1,0:T(8,128)(2,1)}, u32[]{:S(2)}) copy-start(bf16[2048,256]{1,0:T(8,128)(2,1)} %get-tuple-element.11) | copy-start | bytes 3145732

commit v2 on v1

--- a/solution.py
+++ b/solution.py
@@ -21,11 +21,11 @@
 
 
 def exchange_kernel(
-    n_grp, n_fs, n_tp,
-    out_ref, gate_in, up_in, down_in,
-    ret, gate_out, up_out, down_out,
-    piece, hidden, own, pair_send, pair_recv, x_send, x_recv, result,
-    local_sem, slot_s, slot_r, wz_s, wz_r, wy_s, wy_r,
+    n_grp, n_fs, n_tp, capacity,
+    tokens, gain, id_rows, id_cols, group_logits, pair_logits, gate_in, up_in, down_in,
+    mixed, gate_out, up_out, down_out,
+    out_ref, raw, cast, ret, mix, piece, hidden, own, pair_send, pair_recv, x_send, x_recv, result,
+    local_sem, raw_sem, slot_s, slot_r, wz_s, wz_r, wy_s, wy_r,
     gx_s, gx_r, gd_s, gd_r, gf_s, gf_r, pr_s, pr_r, xx_s, xx_r, rt_s, rt_r,
 ):
     g, f, t = lax.axis_index("grp"), lax.axis_index("fs"), lax.axis_index("tp")
@@ -33,7 +33,9 @@
     chip, core = t // 2, lax.rem(t, 2)
     partner = chip * 2 + 1 - core
     width = piece.shape[3]
-    block = gate_in.shape[1]
+    block = cast.shape[2]
+    tok_rows, padded = tokens.shape[0], out_ref.shape[1]
+    experts = n_fs
     share = block // n_grp
 
     def fs_at(k):
@@ -51,6 +53,13 @@
             device_id={axis: peer}, device_id_type=MESH,
         )
 
+    raw_copies = [
+        pltpu.make_async_copy(w, raw.at[m], raw_sem.at[m])
+        for m, w in enumerate((gate_in, up_in, down_in))
+    ]
+    for copy in raw_copies:
+        copy.start()
+
     barrier = pltpu.get_barrier_semaphore()
 
     def greet(axis, peer):
@@ -60,9 +69,41 @@
     each(n_grp - 1, lambda i: greet("grp", grp_at(i + 1)))
     each(n_x - 1, lambda i: greet("tp", chip_at(i + 1) * 2 + core))
     greet("tp", partner)
+
+    def ints(shape, axis):
+        return lax.broadcasted_iota(jnp.int32, shape, axis)
+
+    def route(ids, axis):
+        shape = (experts, tok_rows) if axis == 0 else (tok_rows, experts)
+        named = [(ints(shape, axis) == i).astype(F32) for i in ids]
+        square = (tok_rows, tok_rows)
+        earlier = (ints(square, axis) < ints(square, 1 - axis)).astype(F32).astype(BF16)
+        both = (named[0] + named[1]).astype(BF16)
+        pair = (both, earlier) if axis == 0 else (earlier, both)
+        before = jnp.dot(*pair, preferred_element_type=F32)
+        picks, kept = [], []
+        for i, name in zip(ids, named):
+            rank = jnp.sum(before * name, axis=axis, keepdims=True)
+            kept.append(rank < capacity)
+            slot = i * padded + rank.astype(jnp.int32)
+            picks.append(jnp.where(rank < capacity, slot, -1))
+        return picks, kept
+
+    row_picks, _ = route([id_rows[0:1, :], id_rows[1:2, :]], 0)
+
+    def fill(k):
+        e = fs_at(k)
+        slot = ints((padded, tok_rows), 0) + e * padded
+        named = (slot == row_picks[0]) | (slot == row_picks[1])
+        place = jnp.where(named, 1.0, 0.0).astype(BF16)
+        out_ref[e] = jnp.dot(place, tokens[...], preferred_element_type=F32).astype(BF16)
+
+    each(n_fs - 1, lambda i: fill(i + 1))
     pl.semaphore_wait(barrier, n_fs - 1 + n_grp - 1 + n_x - 1 + 1)
 
-    weights = ((gate_in, gate_out), (up_in, up_out), (down_in, down_out))
+    weights = (
+        (cast.at[0], gate_out), (cast.at[1], up_out), (cast.at[2], down_out)
+    )
 
     def slot_copy(k, source):
         return rcopy(out_ref.at[fs_at(k)], piece.at[t, source], slot_s.at[k],
@@ -72,6 +113,7 @@
         return rcopy(out_ref.at[f], piece.at[t, fs_at(k)], slot_s.at[k], slot_r.at[k], "fs", fs_at(k))
 
     each(n_fs - 1, lambda i: slot_copy(i + 1, f).start())
+    fill(0)
     own_slots = pltpu.make_async_copy(out_ref.at[f], piece.at[t, f], local_sem.at[3])
     own_slots.start()
 
@@ -103,6 +145,15 @@
     own_weights = []
     for m in range(3):
         w_in, w_out = weights[m]
+        raw_copies[m].wait()
+
+        def round_block(e):
+            if m < 2:
+                cast[m, e] = (gain[...] * raw[m, e]).astype(BF16)
+            else:
+                cast[m, e] = raw[m, e].astype(BF16)
+
+        each(n_fs, round_block)
         each(n_fs - 1, lambda i: wz_copy(m, i + 1).start())
         copy = pltpu.make_async_copy(w_in.at[f], w_out.at[pl.ds(f * block, block)], local_sem.at[m])
         copy.start()
@@ -144,6 +195,29 @@
 
     own_slots.wait()
     spread(0)
+
+    ids = [id_cols[:, k : k + 1] for k in range(2)]
+    picks, kept = route(ids, 1)
+    group_exp = jnp.exp(group_logits[...])
+    group_count = group_exp.shape[1]
+    low = ints(group_exp.shape, 1) * (experts // group_count)
+    member = (ids[0] >= low) & (ids[0] < low + experts // group_count)
+    chosen = jnp.sum(jnp.where(member, group_exp, 0.0), axis=1, keepdims=True)
+    chosen = chosen / jnp.sum(group_exp, axis=1, keepdims=True)
+    pair_exp = jnp.exp(pair_logits[...])
+    pair_weight = pair_exp / jnp.sum(pair_exp, axis=1, keepdims=True) * chosen
+    mix_weights = [
+        jnp.where(kept[k], pair_weight[:, k : k + 1], 0.0) for k in range(2)
+    ]
+
+    def blend(k):
+        e = fs_at(k)
+        slot = ints((tok_rows, padded), 1) + e * padded
+        named = (slot == picks[0]) | (slot == picks[1])
+        place = jnp.where(named, 1.0, 0.0).astype(BF16)
+        weight = jnp.where(ids[0] == e, mix_weights[0], 0.0)
+        weight = weight + jnp.where(ids[1] == e, mix_weights[1], 0.0)
+        return jnp.dot(place, ret[e], preferred_element_type=F32) * weight
 
     def spread_arrived(i):
         slot_arrival(i + 1).wait_recv()
@@ -244,7 +318,7 @@
         rt_copy(k).start()
 
     def order(i):
-        return i + 1 if n_fs <= 4 and i + 1 < n_fs else lax.rem(i + 1, n_fs)
+        return (2, 1, 3, 0)[i] if n_fs == 4 else lax.rem(i + 1, n_fs)
 
     stage_pair(order(0))
 
@@ -254,9 +328,17 @@
 
     each(n_fs - 1, pair_and_chip)
     stage_chip(order(n_fs - 1))
-    each(n_fs - 1, lambda i: stage_home(i + 1))
+    each(n_fs - 1, lambda i: stage_home(order(i)))
     ret[f] = total(0)
-    each(n_fs - 1, lambda i: rt_arrival(i + 1).wait_recv())
+    mix[...] = blend(0)
+
+    def collect(i):
+        k = order(i) if n_fs != 4 else (2, 3, 1)[i]
+        rt_arrival(k).wait_recv()
+        mix[...] += blend(k)
+
+    each(n_fs - 1, collect)
+    mixed[...] = mix[...].astype(BF16)
 
     def drain_peer(i):
         k = i + 1
@@ -279,25 +361,36 @@
     each(n_fs, drain_chunk)
 
 
-def exchange(n_grp, n_fs, n_tp, outgoing, gate, up, down):
+def body(
+    tokens, norm_gain, gate_weight, up_weight, down_weight, expert_ids, group_logits, pair_logits
+):
+    n_grp, n_fs, n_tp = (lax.axis_size(a) for a in ("grp", "fs", "tp"))
     n_x = n_tp // 2
-    cap, width = outgoing.shape[1:]
-    block, hid = gate.shape[1:]
+    experts, block, hid = gate_weight.shape
+    tok_rows, width = tokens.shape
+    capacity = 5 * tok_rows * 2 // (4 * experts)
+    cap = -(-capacity // 16) * 16
     vmem = pl.BlockSpec(memory_space=pltpu.VMEM)
+    hbm = pl.BlockSpec(memory_space=pl.ANY)
     dma = pltpu.SemaphoreType.DMA
     matrix = jax.ShapeDtypeStruct((n_fs * block, hid), BF16)
     chunk = (n_fs, n_x, cap, width)
     sem_shapes = [
-        (4,), (n_fs,), (n_fs,), (3, n_fs), (3, n_fs), (3, n_fs, n_grp), (3, n_fs, n_grp),
+        (4,), (3,), (n_fs,), (n_fs,), (3, n_fs), (3, n_fs), (3, n_fs, n_grp), (3, n_fs, n_grp),
         (n_fs, n_x), (n_fs, n_x), (n_fs,), (n_fs,), (n_fs, n_x), (n_fs, n_x),
         (n_fs,), (n_fs,), (n_fs, n_x), (n_fs, n_x), (n_fs,), (n_fs,),
     ]
-    return pl.pallas_call(
-        functools.partial(exchange_kernel, n_grp, n_fs, n_tp),
-        out_shape=(jax.ShapeDtypeStruct((n_fs, cap, width), BF16), matrix, matrix, matrix),
-        in_specs=[vmem] * 4,
+    mixed, *matrices = pl.pallas_call(
+        functools.partial(exchange_kernel, n_grp, n_fs, n_tp, capacity),
+        out_shape=(jax.ShapeDtypeStruct((tok_rows, width), BF16), matrix, matrix, matrix),
+        in_specs=[vmem] * 6 + [hbm] * 3,
         out_specs=(vmem,) * 4,
         scratch_shapes=[
+            pltpu.VMEM((n_fs, cap, width), BF16),
+            pltpu.VMEM((3, n_fs, block, hid), F32),
+            pltpu.VMEM((3, n_fs, block, hid), BF16),
+            pltpu.VMEM((n_fs, cap, width), BF16),
+            pltpu.VMEM((tok_rows, width), F32),
             pltpu.VMEM((n_tp, n_fs, cap, width), BF16),
             pltpu.VMEM((n_fs, cap, hid), BF16),
             pltpu.VMEM(chunk, F32),
@@ -308,60 +401,13 @@
             pltpu.VMEM((n_fs, cap, width), BF16),
         ] + [dma(s) for s in sem_shapes],
         compiler_params=pltpu.CompilerParams(
-            collective_id=0, has_side_effects=True, vmem_limit_bytes=56 * 1024 * 1024
+            collective_id=0, has_side_effects=True, vmem_limit_bytes=48 * 1024 * 1024
         ),
-    )(outgoing, gate, up, down)
-
-
-def body(
-    tokens, norm_gain, gate_weight, up_weight, down_weight, expert_ids, group_logits, pair_logits
-):
-    n_grp, n_fs, n_tp = (lax.axis_size(a) for a in ("grp", "fs", "tp"))
-    experts = gate_weight.shape[0]
-    tok_rows = tokens.shape[0]
-    capacity = 5 * tok_rows * 2 // (4 * experts)
-    padded = -(-capacity // 16) * 16
-    slots = experts * padded
-
-    columns = jnp.arange(experts, dtype=jnp.int32)
-    named = [(expert_ids[:, k, None] == columns[None, :]).astype(F32) for k in range(2)]
-    rows = jnp.arange(tok_rows, dtype=jnp.int32)
-    earlier = (rows[None, :] < rows[:, None]).astype(BF16)
-    before = jnp.dot(earlier, (named[0] + named[1]).astype(BF16), preferred_element_type=F32)
-    picks, kept = [], []
-    for k in range(2):
-        rank = jnp.sum(before * named[k], axis=1).astype(jnp.int32)
-        kept.append(rank < capacity)
-        picks.append(jnp.where(kept[k], expert_ids[:, k] * padded + rank, slots))
-    slot_ids = jnp.arange(slots, dtype=jnp.int32)
-    place = [(picks[k][:, None] == slot_ids[None, :]).astype(BF16) for k in range(2)]
-    outgoing = lax.dot_general(
-        place[0] + place[1], tokens, (((0,), (0,)), ((), ())), preferred_element_type=F32
-    ).astype(BF16).reshape(experts, padded, -1)
-
-    scaled = norm_gain[None, :, None]
-    gate_cast = (scaled * gate_weight).astype(BF16)
-    up_cast = (scaled * up_weight).astype(BF16)
-    down_cast = down_weight.astype(BF16)
-    returned, gate_here, up_here, down_here = exchange(
-        n_grp, n_fs, n_tp, outgoing, gate_cast, up_cast, down_cast
+    )(
+        tokens, norm_gain[:, None], expert_ids.T, expert_ids, group_logits, pair_logits,
+        gate_weight, up_weight, down_weight,
     )
-    returned = returned.reshape(slots, -1)
-
-    group_exp = jnp.exp(group_logits)
-    group_count = group_logits.shape[1]
-    group_pick = expert_ids[:, 0] // (experts // group_count)
-    groups = jnp.arange(group_count, dtype=jnp.int32)
-    chosen = jnp.sum(jnp.where(groups[None, :] == group_pick[:, None], group_exp, 0.0), axis=1)
-    chosen = chosen / jnp.sum(group_exp, axis=1)
-    pair_exp = jnp.exp(pair_logits)
-    weights = pair_exp / jnp.sum(pair_exp, axis=1, keepdims=True) * chosen[:, None]
-    mixed = 0.0
-    for k in range(2):
-        weight = weights[:, k] * kept[k].astype(F32)
-        picked = jnp.dot(place[k], returned, preferred_element_type=F32)
-        mixed = mixed + picked * weight[:, None]
-    return (mixed.astype(BF16), gate_here[None], up_here[None], down_here[None])
+    return (mixed, *(m[None] for m in matrices))
 
 
 def solution(mesh):

time: 133 us -> 115 us (0.86)
  the two profiles are of different devices: /device:TPU:29 before, /device:TPU:0 now
where the time goes in v2:
time: 115 us
  Pallas kernels  106 us (92%)
  local copies, waits for them, and re-layouts  8.61 us (7%)
    pallas_call x1, Pallas kernels, body(): pl.pallas_call(functools.partial(exchange_kernel, n_grp, n_fs, n_tp, capa...  106 us
    unnamed x11, local copies, waits for them, and re-layouts  7.79 us

profile of v2, /device:TPU:0, one launch (start us, length us, event | category | flops | bytes accessed | tf_op | source)
XLA Modules:
  0.0 114.8 jit_solution(1921792178701050205)
XLA Ops:
  0.6 0.8 copy.17.group_logits
  1.5 0.8 copy.18.pair_logits
  2.3 0.8 copy.16.id_cols
  3.1 0.8 copy.15.gain
  3.9 0.0 copy-start
  4.0 1.0 copy-done
  4.9 0.0 copy-start.1
  4.9 0.7 copy-done.1
  5.6 105.5 %shard_map.111 = (bf16[384,512]{1,0:T(8,128)(2,1)S(1)}, bf16[2048,256]{1,0:T(8,128)(2,1)S(1)}, bf16[2048,256]{1,0:T(8,128)(2,1)S(1)}, bf16[2048,256]{1,0:T(8,128)(2,1)S(1)}) custom-call(bf16[384,512]{1,0:T(8,128)(2,1)S(1)} %copy-done, f32[512,1]{1,0:T(8,128)S(1)} %copy.15.gain, s32[2,384]{1,0:T(2,128)S(1)} %bitcast.8, s32[384,2]{1,0:T(8,128)S(1)} %copy.16.id_cols, ...), custom_call_target="tpu_custom_call" | custom-call | tf_op jit(solution)/shard_map/pallas_call | solution.py:383
  111.2 0.7 copy.23
  111.9 1.0 copy.24
  112.9 1.0 copy.25
  113.9 1.0 copy.26
Async XLA Ops:
  3.9 1.0 copy-start
  4.9 0.7 copy-start.1

commit v3 on v2

--- a/solution.py
+++ b/solution.py
@@ -22,7 +22,7 @@
 
 def exchange_kernel(
     n_grp, n_fs, n_tp, capacity,
-    tokens, gain, id_rows, id_cols, group_logits, pair_logits, gate_in, up_in, down_in,
+    tokens, gain, id_rows, group_logits, pair_logits, gate_in, up_in, down_in,
     mixed, gate_out, up_out, down_out,
     out_ref, raw, cast, ret, mix, piece, hidden, own, pair_send, pair_recv, x_send, x_recv, result,
     local_sem, raw_sem, slot_s, slot_r, wz_s, wz_r, wy_s, wy_r,
@@ -40,6 +40,16 @@
 
     def fs_at(k):
         return lax.rem(f + k, n_fs)
+
+    def outward(i):
+        return jnp.where(f < n_fs // 2, i + 1, n_fs - 1 - i)
+
+    def nearest(i):
+        if n_fs != 4:
+            return outward(i)
+        first = jnp.where(f % 2 == 0, 1, 3)
+        last = jnp.where(f == 0, 3, jnp.where(f == 3, 1, 2))
+        return (first, 6 - first - last, last)[i]
 
     def grp_at(k):
         return lax.rem(g + k, n_grp)
@@ -112,7 +122,7 @@
     def slot_arrival(k):
         return rcopy(out_ref.at[f], piece.at[t, fs_at(k)], slot_s.at[k], slot_r.at[k], "fs", fs_at(k))
 
-    each(n_fs - 1, lambda i: slot_copy(i + 1, f).start())
+    each(n_fs - 1, lambda i: slot_copy(outward(i), f).start())
     fill(0)
     own_slots = pltpu.make_async_copy(out_ref.at[f], piece.at[t, f], local_sem.at[3])
     own_slots.start()
@@ -154,10 +164,12 @@
                 cast[m, e] = raw[m, e].astype(BF16)
 
         each(n_fs, round_block)
-        each(n_fs - 1, lambda i: wz_copy(m, i + 1).start())
         copy = pltpu.make_async_copy(w_in.at[f], w_out.at[pl.ds(f * block, block)], local_sem.at[m])
         copy.start()
         own_weights.append(copy)
+
+    for m in range(3):
+        each(n_fs - 1, lambda i: wz_copy(m, outward(i)).start())
 
     def forward(m, k):
         wz_arrival(m, k).wait_recv()
@@ -196,15 +208,16 @@
     own_slots.wait()
     spread(0)
 
+    id_cols = jnp.transpose(id_rows[...])
     ids = [id_cols[:, k : k + 1] for k in range(2)]
     picks, kept = route(ids, 1)
-    group_exp = jnp.exp(group_logits[...])
+    group_exp = jnp.exp(jnp.transpose(group_logits[...]))
     group_count = group_exp.shape[1]
     low = ints(group_exp.shape, 1) * (experts // group_count)
     member = (ids[0] >= low) & (ids[0] < low + experts // group_count)
     chosen = jnp.sum(jnp.where(member, group_exp, 0.0), axis=1, keepdims=True)
     chosen = chosen / jnp.sum(group_exp, axis=1, keepdims=True)
-    pair_exp = jnp.exp(pair_logits[...])
+    pair_exp = jnp.exp(jnp.transpose(pair_logits[...]))
     pair_weight = pair_exp / jnp.sum(pair_exp, axis=1, keepdims=True) * chosen
     mix_weights = [
         jnp.where(kept[k], pair_weight[:, k : k + 1], 0.0) for k in range(2)
@@ -220,8 +233,8 @@
         return jnp.dot(place, ret[e], preferred_element_type=F32) * weight
 
     def spread_arrived(i):
-        slot_arrival(i + 1).wait_recv()
-        spread(i + 1)
+        slot_arrival(nearest(i)).wait_recv()
+        spread(nearest(i))
 
     each(n_fs - 1, spread_arrived)
 
@@ -232,12 +245,10 @@
 
     hand_over(0)
 
-    def hand_and_forward(i):
-        hand_over(i + 1)
-        forward(0, i + 1)
-
-    each(n_fs - 1, hand_and_forward)
-    each(n_fs - 1, lambda i: forward(1, i + 1))
+    each(n_fs - 1, lambda i: hand_over(nearest(i)))
+
+    for m in range(3):
+        each(n_fs - 1, lambda i: forward(m, nearest(i)))
 
     def all_in(m):
         own_weights[m].wait()
@@ -262,12 +273,7 @@
             up = up_part if up is None else up + up_part
         hidden[k] = (gate / (1.0 + jnp.exp(-gate)) * up).astype(BF16)
 
-    def hidden_and_forward(i):
-        make_hidden(i + 1)
-        forward(2, i + 1)
-
-    each(n_fs - 1, hidden_and_forward)
-    make_hidden(0)
+    each(n_fs, lambda i: make_hidden(i))
     all_in(2)
 
     def term(k, j, to_core):
@@ -318,7 +324,7 @@
         rt_copy(k).start()
 
     def order(i):
-        return (2, 1, 3, 0)[i] if n_fs == 4 else lax.rem(i + 1, n_fs)
+        return lax.rem(outward(i) + n_fs, n_fs)
 
     stage_pair(order(0))
 
@@ -333,7 +339,7 @@
     mix[...] = blend(0)
 
     def collect(i):
-        k = order(i) if n_fs != 4 else (2, 3, 1)[i]
+        k = nearest(i)
         rt_arrival(k).wait_recv()
         mix[...] += blend(k)
 
@@ -383,7 +389,7 @@
     mixed, *matrices = pl.pallas_call(
         functools.partial(exchange_kernel, n_grp, n_fs, n_tp, capacity),
         out_shape=(jax.ShapeDtypeStruct((tok_rows, width), BF16), matrix, matrix, matrix),
-        in_specs=[vmem] * 6 + [hbm] * 3,
+        in_specs=[vmem] * 5 + [hbm] * 3,
         out_specs=(vmem,) * 4,
         scratch_shapes=[
             pltpu.VMEM((n_fs, cap, width), BF16),
@@ -404,7 +410,7 @@
             collective_id=0, has_side_effects=True, vmem_limit_bytes=48 * 1024 * 1024
         ),
     )(
-        tokens, norm_gain[:, None], expert_ids.T, expert_ids, group_logits, pair_logits,
+        tokens, norm_gain[:, None], expert_ids.T, group_logits.T, pair_logits.T,
         gate_weight, up_weight, down_weight,
     )
     return (mixed, *(m[None] for m in matrices))

time: 115 us -> 112 us (0.974)
  Pallas kernels: 106 us -> 104 us
    pallas_call x1, Pallas kernels: 106 us -> 104 us  [body(): pl.pallas_call(functools.partial(exchange_kernel, n_grp, n_fs, n_tp, capa...]
    unnamed x11 -> x12, local copies, waits for them, and re-layouts: 7.79 us -> 6.7 us
where the time goes in v3:
time: 112 us
  Pallas kernels  104 us (93%)
  local copies, waits for them, and re-layouts  7.52 us (7%)
    pallas_call x1, Pallas kernels, body(): pl.pallas_call(functools.partial(exchange_kernel, n_grp, n_fs, n_tp, capa...  104 us
    unnamed x12, local copies, waits for them, and re-layouts  6.7 us

profile of v3, /device:TPU:0, one launch (start us, length us, event | category | flops | bytes accessed | tf_op | source)
XLA Modules:
  0.0 112.1 jit_solution(13677565775381111622)
XLA Ops:
  0.6 0.8 copy.12.gain
  1.5 0.0 copy-start
  1.5 1.0 copy-done
  2.5 0.0 copy-start.1
  2.5 0.7 copy-done.1
  3.1 0.0 copy-start.2
  3.1 0.7 copy-done.2
  3.8 0.0 copy-start.3
  3.8 0.7 copy-done.3
  4.5 103.9 %shard_map.111 = (bf16[384,512]{1,0:T(8,128)(2,1)S(1)}, bf16[2048,256]{1,0:T(8,128)(2,1)S(1)}, bf16[2048,256]{1,0:T(8,128)(2,1)S(1)}, bf16[2048,256]{1,0:T(8,128)(2,1)S(1)}) custom-call(bf16[384,512]{1,0:T(8,128)(2,1)S(1)} %copy-done, f32[512,1]{1,0:T(8,128)S(1)} %copy.12.gain, s32[2,384]{1,0:T(2,128)S(1)} %bitcast.10, f32[2,384]{1,0:T(2,128)S(1)} %bitcast.11, ...), custom_call_target="tpu_custom_call" | custom-call | tf_op jit(solution)/shard_map/pallas_call | solution.py:389
  108.4 0.7 copy.17
  109.2 1.0 copy.18
  110.2 1.0 copy.19
  111.1 1.0 copy.20
Async XLA Ops:
  1.5 1.0 copy-start
  2.5 0.7 copy-start.1
  3.1 0.7 copy-start.2
  3.8 0.7 copy-start.3
